TPU v7x, 32 devices: a whole 2x2x4 slice. The times are simulated.
32 devices in a mesh: fs: 8 (over z, y), tp: 4 (over x, core).
Axes of the slice: x: 2, y: 2, z: 4, core: 2. Of those that a mesh axis runs over, the one named last changes fastest.
Arguments:
- tokens: bfloat16 [8192, 2048], P('fs'), may hold values from -6 to 6
- norm_gain: float32 [2048], P('fs'), may hold values from 0.1 to 1.9
- gate_train: float32 [8, 2048, 768], P(None, 'fs', 'tp'), may hold values from -0.125 to 0.125
- up_train: float32 [8, 2048, 768], P(None, 'fs', 'tp'), may hold values from -0.125 to 0.125
- down_train: float32 [8, 768, 2048], P(None, 'fs', 'tp'), may hold values from -0.21875 to 0.21875
- expert_ids: int32 [8192, 2], P('fs'), may hold values from 0 to 7, all different within a row; in each aligned block of 1024 rows (0 to 1023, 1024 to 2047, ...) at most 512 rows name the same one
- route_weights: float32 [8192, 2], P('fs'), may hold values from 0.1 to 1
Outputs:
- gate_serve: bfloat16 [8, 2048, 768], P('fs', None, 'tp')
- up_serve: bfloat16 [8, 2048, 768], P('fs', None, 'tp')
- down_serve: bfloat16 [8, 768, 2048], P('fs', 'tp')
- mixed: bfloat16 [8192, 2048], P('fs', 'tp')
Inputs may be any that keep to these rules, and one draw needn't show every extreme that they name: `expert_ids`: each row names 2 different experts. Within each aligned block of 1024 rows no expert is named more than 512 times, and in every block some expert is named exactly 512 times; every expert is named somewhere.
All inputs are finite; a program needn't handle non-finite values.
Results may differ from a plain program's by a relative error of at most 0.011.
Values may be sent and summed in bfloat16 or wider, within the bound.
A program may use at most 128 MiB of HBM per device.

v0:
```python
import jax
import jax.numpy as jnp
from jax import lax
from jax.sharding import PartitionSpec as P

epsilon = 1e-06


def on_device(tokens, norm_gain, gate_train, up_train, down_train, expert_ids, route_weights):
    experts, rows, cols = gate_train.shape
    fs_at = lax.axis_index("fs")
    tok_rows, picks = expert_ids.shape
    down_rows, down_cols = down_train.shape[1:]
    fs_count = lax.axis_size("fs")
    gate_up = jnp.concatenate(
        [norm_gain[None, :, None] * gate_train, norm_gain[None, :, None] * up_train], axis=2
    ).astype(jnp.bfloat16)
    gate_up = gate_up.transpose(1, 0, 2).reshape(rows, experts * 2 * cols)
    gate_up_all = lax.all_gather(gate_up, "fs", axis=0, tiled=True)
    down_all = lax.all_gather(
        down_train.astype(jnp.bfloat16).reshape(experts * down_rows, down_cols),
        "fs",
        axis=0,
        tiled=True,
    )
    tok_float = tokens.astype(jnp.float32)
    normed = (
        tok_float * lax.rsqrt(jnp.mean(tok_float * tok_float, axis=-1, keepdims=True) + epsilon)
    ).astype(jnp.bfloat16)
    shares = route_weights / jnp.sum(route_weights, axis=-1, keepdims=True)
    group = 2 * lax.axis_size("tp")
    picked = [jnp.zeros((tok_rows, cols), jnp.float32) for _ in range(picks)]
    for first in range(0, experts, group):
        part = gate_up_all[:, first * 2 * cols : (first + group) * 2 * cols]
        if first:
            part, picked = lax.optimization_barrier((part, picked))
        acts = jnp.dot(normed, part, preferred_element_type=jnp.float32)
        for at in range(group):
            g = acts[:, at * 2 * cols : at * 2 * cols + cols]
            u = acts[:, at * 2 * cols + cols : (at + 1) * 2 * cols]
            h = jax.nn.silu(g) * u
            for k in range(picks):
                picked[k] = picked[k] + jnp.where(expert_ids[:, k : k + 1] == first + at, h, 0.0)
    hidden = jnp.stack([picked[k] * shares[:, k : k + 1] for k in range(picks)], 0)
    hidden_all = lax.all_gather(hidden.astype(jnp.bfloat16), "tp", axis=2, tiled=True)
    hidden_all = hidden_all.reshape(picks, tok_rows, fs_count, 1, down_rows)
    ids = jnp.arange(experts, dtype=jnp.int32)[None, None, :, None]
    mixed = jnp.zeros((tok_rows, down_cols), jnp.float32)
    for first in range(0, fs_count, group):
        blocks = hidden_all[:, :, first : first + group]
        if first:
            blocks, mixed = lax.optimization_barrier((blocks, mixed))
        spread = jnp.zeros((tok_rows, group, experts, down_rows), jnp.bfloat16)
        for k in range(picks):
            spread = jnp.where(expert_ids[:, k][:, None, None, None] == ids, blocks[k], spread)
        depth = experts * down_rows
        mixed = mixed + jnp.dot(
            spread.reshape(tok_rows, group * depth),
            down_all[first * depth : (first + group) * depth],
            preferred_element_type=jnp.float32,
        )
    mixed = mixed.astype(jnp.bfloat16)
    own = lax.dynamic_slice_in_dim(gate_up_all, fs_at * 2 * cols, 2 * cols, 1)
    down_own = lax.dynamic_slice_in_dim(
        down_all.reshape(fs_count, experts, down_rows, down_cols), fs_at, 1, 1
    ).reshape(1, fs_count * down_rows, down_cols)
    down_serve = lax.all_to_all(down_own, "tp", split_axis=1, concat_axis=2, tiled=True)
    return (own[None, :, :cols], own[None, :, cols:], down_serve, mixed)


def solution(mesh):
    return jax.shard_map(
        on_device,
        mesh=mesh,
        in_specs=(
            P("fs", None),
            P("fs"),
            P(None, "fs", "tp"),
            P(None, "fs", "tp"),
            P(None, "fs", "tp"),
            P("fs", None),
            P("fs", None),
        ),
        out_specs=(P("fs", None, "tp"), P("fs", None, "tp"), P("fs", "tp", None), P("fs", "tp")),
        check_vma=False,
    )
```

profile of v0, /device:TPU:0, one launch (start us, length us, event | category | flops | bytes accessed | tf_op | source)
XLA Modules:
  0.0 353.5 jit_solution(751838854216082823)
XLA Ops:
  7.2 0.0 all-gather.4.cloned.1.call-start
  7.2 2.3 multiply_convert_fusion.1
  9.6 1.3 pad_maximum_fusion
  10.9 0.0 all-gather.6.cloned.1.call-start
  10.9 1.0 convert_element_type.14
  11.9 0.0 all-gather.8.cloned.1.call-start
  12.0 0.2 compare_reduce_fusion.15
  12.2 3.1 fusion
  15.4 174.5 %all-gather.4.cloned.1.call-done = bf16[2048,3072]{0,1:T(8,128)(2,1)} async-done(((bf16[256,3072]{0,1:T(8,128)(2,1)}), bf16[2048,3072]{0,1:T(8,128)(2,1)}) %all-gather.4.cloned.1.call-update) | async-done | bytes 12582928 | tf_op jit(solution)/shard_map/all_gather | solution.py:19
  189.9 17.1 %fusion.2 = f32[1024,3072]{1,0:T(8,128)S(1)} fusion(bf16[2048,3072]{0,1:T(8,128)(2,1)} %all-gather.4.cloned.1.call-done, bf16[1024,2048]{1,0:T(8,128)(2,1)} %param.7, f32[1024]{0:T(1024)S(1)} %add_rsqrt_fusion), kind=kOutput, calls=%fused_computation.5 | convolution fusion | flops 12891193344 | bytes 29364224 | tf_op jit(solution)/shard_map/dot_general | solution.py:37
  207.0 4.5 %fusion.5 = bf16[1,1024,192]{2,1,0:T(8,128)(2,1)S(1)} fusion(f32[1024]{0:T(1024)S(1)} %bitcast.47, pred[1024]{0:T(1024)(128)(4,1)S(1)} %get-tuple-element.19, pred[1024]{0:T(1024)(128)(4,1)S(1)} %get-tuple-element.18, pred[1024]{0:T(1024)(128)(4,1)S(1)} %get-tuple-element.17, pred[1024]{0:T(1024)(128)(4,1)S(1)} %get-tuple-element.16, ...), kind=kLoop, calls=%fused_computation.24 | loop fusion | flops 11206656 | bytes 12988416 | tf_op jit(solution)/shard_map/stack | solution.py:44
  211.5 4.5 %fusion.6 = bf16[1,1024,192]{2,1,0:T(8,128)(2,1)S(1)} fusion(f32[1024]{0:T(1024)S(1)} %bitcast.46, pred[1024]{0:T(1024)(128)(4,1)S(1)} %get-tuple-element.12, pred[1024]{0:T(1024)(128)(4,1)S(1)} %get-tuple-element.11, pred[1024]{0:T(1024)(128)(4,1)S(1)} %get-tuple-element.10, pred[1024]{0:T(1024)(128)(4,1)S(1)} %get-tuple-element.9, ...), kind=kLoop, calls=%fused_computation.25 | loop fusion | flops 11206656 | bytes 12988416 | tf_op jit(solution)/shard_map/stack | solution.py:44
  216.0 0.2 pad_maximum_fusion.1
  216.2 2.0 copy.22
  218.2 71.3 %all-gather.6.cloned.1.call-done = bf16[6144,512]{1,0:T(8,128)(2,1)} async-done(((bf16[768,512]{1,0:T(8,128)(2,1)}), bf16[6144,512]{1,0:T(8,128)(2,1)}) %all-gather.6.cloned.1.call-update) | async-done | bytes 6291472 | tf_op jit(solution)/shard_map/all_gather | solution.py:20
  289.5 1.2 constant_dynamic-slice_fusion
  290.8 1.2 copy.30
  292.0 0.5 broadcast.126
  292.5 5.4 %reduce.32 = bf16[768,512]{1,0:T(8,128)(2,1)S(1)} reduce(bf16[768,1,512]{2,1,0:T(2,128)(2,1)S(1)} %bitcast.37, bf16[]{:T(256)} %broadcast.126), dimensions={1}, to_apply=%bitcast.32.reduce_sub_computation | reduce | bytes 1572866
  297.9 1.4 reshape.117
  299.3 3.7 %all-to-all-start = ((bf16[4,2,49152]{2,1,0:T(2,128)(2,1)}), bf16[4,2,49152]{2,1,0:T(2,128)(2,1)S(1)}, u32[]{:S(2)}, u32[]{:S(2)}) async-start(bf16[4,2,49152]{2,1,0:T(2,128)(2,1)} %reshape.117), calls=%async_computation | async-start | bytes 1572864 | tf_op jit(solution)/shard_map/all_to_all | solution.py:67
  303.0 20.2 %all-to-all-done = bf16[4,2,49152]{2,1,0:T(2,128)(2,1)S(1)} async-done(((bf16[4,2,49152]{2,1,0:T(2,128)(2,1)}), bf16[4,2,49152]{2,1,0:T(2,128)(2,1)S(1)}, u32[]{:S(2)}, u32[]{:S(2)}) %all-to-all-start) | async-done | bytes 786464 | tf_op jit(solution)/shard_map/all_to_all | solution.py:67
  323.2 0.7 reshape.118
  324.0 0.2 copy.25
  324.2 1.0 copy.28
  325.2 2.7 dynamic-slice_bitcast_fusion
  327.9 7.8 %fusion.7 = (bf16[1,1024,768]{1,0,2:T(2,128)(2,1)S(1)}, bf16[1,1024,768]{1,0,2:T(2,128)(2,1)S(1)}) fusion(bf16[2,1024,768]{1,0,2:T(2,128)(2,1)} %all-gather.8.cloned.1.call-done), kind=kLoop, calls=%fused_computation.47 | loop fusion | bytes 6291456 | tf_op jit(solution)/shard_map/slice | solution.py:55
  335.7 0.6 copy.26
  336.3 0.6 copy.27
  336.9 1.9 select_select_fusion
  338.8 0.5 slice-done.1
  339.3 7.6 %convolution_convert_fusion = bf16[1024,512]{1,0:T(8,128)(2,1)} fusion(bf16[1024,6144]{0,1:T(8,128)(2,1)S(1)} %bitcast.33, bf16[6144,512]{1,0:T(8,128)(2,1)S(1)} %bitcast.45), kind=kOutput, calls=%fused_computation.10 | convolution fusion | flops 6442975232 | bytes 19922944 | tf_op jit(solution)/shard_map/dot_general | solution.py:57
  (20 shorter events, 0.1 us)
Async XLA Ops:
  7.2 3.8 %copy-start = (f32[8,96,512]{2,1,0:T(8,128)S(1)}, f32[8,96,512]{2,1,0:T(8,128)}, u32[]{:S(2)}) copy-start(f32[8,96,512]{2,1,0:T(8,128)} %param.11) | copy-start | bytes 4718596
  7.2 182.7 %all-gather.4.cloned.1.call-start = ((), (), s32[]{:S(2)}) async-start(), calls=%async_computation.1 | async-start | bytes 14155776 | tf_op jit(solution)/shard_map/all_gather | solution.py:19
  9.6 2.4 copy-start.2
  9.6 2.5 copy-start.1
  10.9 278.7 %all-gather.6.cloned.1.call-start = ((), (), s32[]{:S(2)}) async-start(), calls=%async_computation.2 | async-start | bytes 7077888 | tf_op jit(solution)/shard_map/all_gather | solution.py:20
  11.9 315.9 %all-gather.8.cloned.1.call-start = ((), (), s32[]{:S(2)}) async-start(), calls=%async_computation.3 | async-start | bytes 3932160 | tf_op jit(solution)/shard_map/all_gather | solution.py:45
  299.3 23.9 %all-to-all-start = ((bf16[4,2,49152]{2,1,0:T(2,128)(2,1)}), bf16[4,2,49152]{2,1,0:T(2,128)(2,1)S(1)}, u32[]{:S(2)}, u32[]{:S(2)}) async-start(bf16[4,2,49152]{2,1,0:T(2,128)(2,1)} %reshape.117), calls=%async_computation | async-start | bytes 1572864 | tf_op jit(solution)/shard_map/all_to_all | solution.py:67
  336.3 2.5 slice-start
  336.9 2.4 slice-start.1
Sparse Core Ops, SparseCore 0:
  11.0 178.8 all-gather.3
  192.6 96.8 all-gather.5
  291.7 35.1 all-gather.7
where the time goes:
time: 354 us; the launch traced here: 353 us
  waiting for transfers between devices  266 us (75%)
  matrix products  24.7 us (7%)
  other arithmetic  24.4 us (7%)
  local copies, waits for them, and re-layouts  20.5 us (6%)
  between operations  14 us (4%)
  starting transfers between devices  3.8 us (1%)
    all_gather x1, waiting for transfers between devices, on_device(): gate_up_all = lax.all_gather(gate_up, 'fs', axis=0, tiled=True)  175 us
    all_gather x1, waiting for transfers between devices, on_device(): lax.all_gather(down_train.astype(jnp.bfloat16).reshape(experts * down_row...  71.3 us
    all_to_all x1, waiting for transfers between devices, on_device(): lax.all_to_all(down_own, 'tp', split_axis=1, concat_axis=2, tiled=True)  20.2 us
    dot_general x1, matrix products, on_device(): acts = jnp.dot(normed, part, preferred_element_type=jnp.float32)  17.1 us
    another operation x3, other arithmetic, on_device(): jnp.stack([picked[k] * shares[:, k:k + 1] for k in range(picks)], 0)  9.18 us
    slice x1, local copies, waits for them, and re-layouts, on_device(): blocks[k]  7.82 us
    dot_general x1, matrix products, on_device(): jnp.dot(spread.reshape(tok_rows, group * depth), down_all[first * depth:(...  7.64 us
  transfers between devices with their start and end apart: 4, of which 3 were waited for; matrix products, arithmetic and copies ran while one was open for 13% of the time, Pallas kernels for 0%

commit v1 on v0

--- a/solution.py
+++ b/solution.py
@@ -16,7 +16,25 @@
         [norm_gain[None, :, None] * gate_train, norm_gain[None, :, None] * up_train], axis=2
     ).astype(jnp.bfloat16)
     gate_up = gate_up.transpose(1, 0, 2).reshape(rows, experts * 2 * cols)
-    gate_up_all = lax.all_gather(gate_up, "fs", axis=0, tiled=True)
+    count, here, extent = (lax.axis_size("fs"), lax.axis_index("fs"), gate_up.shape[0])
+    ahead = [(i, (i + 1) % count) for i in range(count)]
+    behind = [(i, (i - 1) % count) for i in range(count)]
+    gate_up_all = jnp.zeros(
+        (*gate_up.shape[:0], count * extent, *gate_up.shape[0 + 1 :]), gate_up.dtype
+    )
+    gate_up_all = lax.dynamic_update_slice_in_dim(gate_up_all, gate_up, here * extent, axis=0)
+    from_left = from_right = gate_up
+    halfway = count // 2
+    for step in range(1, halfway + 1):
+        from_left = lax.ppermute(from_left, "fs", ahead)
+        gate_up_all = lax.dynamic_update_slice_in_dim(
+            gate_up_all, from_left, (here - step) % count * extent, axis=0
+        )
+        if step < count - halfway:
+            from_right = lax.ppermute(from_right, "fs", behind)
+            gate_up_all = lax.dynamic_update_slice_in_dim(
+                gate_up_all, from_right, (here + step) % count * extent, axis=0
+            )
     down_all = lax.all_gather(
         down_train.astype(jnp.bfloat16).reshape(experts * down_rows, down_cols),
         "fs",

time: 354 us -> 453 us (1.28)
  waiting for transfers between devices: 266 us -> 319 us
  local copies, waits for them, and re-layouts: 20.5 us -> 45.2 us
  starting transfers between devices: 3.8 us -> 25.6 us
    ppermute x0 -> x7, waiting for transfers between devices: none -> 203 us  [the longest x4 203 us: on_device(): from_left = lax.ppermute(from_left, 'fs', ahead)]
    all_gather x1 -> x0, waiting for transfers between devices: 175 us -> none  [on_device(): gate_up_all = lax.all_gather(gate_up, 'fs', axis=0, tiled=True)]
    all_gather x1, waiting for transfers between devices: 0.01 us -> 23.1 us  [on_device(): lax.all_gather(hidden.astype(jnp.bfloat16), 'tp', axis=2, tiled=True)]
    all_gather x1, waiting for transfers between devices: 71.3 us -> 92.5 us  [on_device(): lax.all_gather(down_train.astype(jnp.bfloat16).reshape(experts * down_row...]
    ppermute x0 -> x7, starting transfers between devices: none -> 21 us  [the longest x4 10.6 us: on_device(): from_left = lax.ppermute(from_left, 'fs', ahead)]
    all_to_all x1, waiting for transfers between devices: 20.2 us -> 0.01 us  [on_device(): lax.all_to_all(down_own, 'tp', split_axis=1, concat_axis=2, tiled=True)]
    dynamic_update_slice x0 -> x8, local copies, waits for them, and re-layouts: none -> 15.2 us  [the longest x4 8.18 us: on_device(): lax.dynamic_update_slice_in_dim(gate_up_all, from_left, (here - step) % c...]
    broadcast_in_dim x0 -> x1, local copies, waits for them, and re-layouts: none -> 6.18 us  [on_device(): jnp.zeros((*gate_up.shape[:0], count * extent, *gate_up.shape[0 + 1:]), g...]
  transfers between devices with their start and end apart: 4 -> 10, of which waited for: 3 -> 6; matrix products, arithmetic and copies ran while one was open for 13% -> 10% of each run, Pallas kernels for 0% -> 0%
where the time goes in v1:
time: 453 us
  waiting for transfers between devices  319 us (70%)
  local copies, waits for them, and re-layouts  45.2 us (10%)
  matrix products  25.7 us (6%)
  starting transfers between devices  25.6 us (6%)
  other arithmetic  23 us (5%)
  between operations  14.4 us (3%)
    ppermute x4, waiting for transfers between devices, on_device(): from_left = lax.ppermute(from_left, 'fs', ahead)  203 us
    all_gather x1, waiting for transfers between devices, on_device(): lax.all_gather(down_train.astype(jnp.bfloat16).reshape(experts * down_row...  92.5 us
    all_gather x1, waiting for transfers between devices, on_device(): lax.all_gather(hidden.astype(jnp.bfloat16), 'tp', axis=2, tiled=True)  23.1 us
    dot_general x1, matrix products, on_device(): acts = jnp.dot(normed, part, preferred_element_type=jnp.float32)  15.8 us
    ppermute x4, starting transfers between devices, on_device(): from_left = lax.ppermute(from_left, 'fs', ahead)  10.6 us
    ppermute x3, starting transfers between devices, on_device(): from_right = lax.ppermute(from_right, 'fs', behind)  10.4 us
    dot_general x1, matrix products, on_device(): jnp.dot(spread.reshape(tok_rows, group * depth), down_all[first * depth:(...  9.89 us
    another operation x3, other arithmetic, on_device(): jnp.stack([picked[k] * shares[:, k:k + 1] for k in range(picks)], 0)  9.2 us
  transfers between devices with their start and end apart: 10, of which 6 were waited for; matrix products, arithmetic and copies ran while one was open for 10% of the time, Pallas kernels for 0%

profile of v1, /device:TPU:0, one launch (start us, length us, event | category | flops | bytes accessed | tf_op | source)
XLA Modules:
  0.0 452.7 jit_solution(14677355470906214042)
XLA Ops:
  7.2 2.4 multiply_convert_fusion.1
  9.8 3.0 collective-permute-start
  12.8 3.1 collective-permute-start.1
  15.9 64.3 %collective-permute-done = bf16[256,3072]{0,1:T(8,128)(2,1)S(1)} collective-permute-done((bf16[256,3072]{0,1:T(8,128)(2,1)S(1)}, bf16[256,3072]{0,1:T(8,128)(2,1)S(1)}, u32[]{:S(2)}, u32[]{:S(2)}) %collective-permute-start) | collective-permute-done | bytes 1572896 | tf_op jit(solution)/shard_map/ppermute | solution.py:29
  80.2 2.5 collective-permute-start.2
  82.6 4.2 collective-permute-start.3
  86.9 62.3 %collective-permute-done.2 = bf16[256,3072]{0,1:T(8,128)(2,1)} collective-permute-done((bf16[256,3072]{0,1:T(8,128)(2,1)S(1)}, bf16[256,3072]{0,1:T(8,128)(2,1)}, u32[]{:S(2)}, u32[]{:S(2)}) %collective-permute-start.2) | collective-permute-done | bytes 1572896 | tf_op jit(solution)/shard_map/ppermute | solution.py:29
  149.1 2.6 collective-permute-start.4
  153.0 6.2 %broadcast_in_dim.181 = bf16[2048,3072]{0,1:T(8,128)(2,1)} broadcast(bf16[]{:T(256)} %constant.75.clone.1), dimensions={} | broadcast | bytes 12582914 | tf_op jit(solution)/shard_map/broadcast_in_dim | solution.py:22
  160.6 3.0 collective-permute-start.5
  165.0 52.7 %collective-permute-done.4 = bf16[256,3072]{0,1:T(8,128)(2,1)} collective-permute-done((bf16[256,3072]{0,1:T(8,128)(2,1)}, bf16[256,3072]{0,1:T(8,128)(2,1)}, u32[]{:S(2)}, u32[]{:S(2)}) %collective-permute-start.4) | collective-permute-done | bytes 1572896 | tf_op jit(solution)/shard_map/ppermute | solution.py:29
  217.7 2.5 collective-permute-start.6
  220.2 1.4 constant_dynamic-update-slice_fusion.5
  221.6 2.7 constant_dynamic-update-slice_fusion.4
  224.3 2.9 constant_dynamic-update-slice_fusion.3
  227.2 2.8 constant_dynamic-update-slice_fusion.2
  231.3 23.9 %collective-permute-done.6 = bf16[256,3072]{0,1:T(8,128)(2,1)S(1)} collective-permute-done((bf16[256,3072]{0,1:T(8,128)(2,1)}, bf16[256,3072]{0,1:T(8,128)(2,1)S(1)}, u32[]{:S(2)}, u32[]{:S(2)}) %collective-permute-start.6) | collective-permute-done | bytes 1572896 | tf_op jit(solution)/shard_map/ppermute | solution.py:29
  256.6 15.8 %fusion.2 = f32[1024,3072]{1,0:T(8,128)S(1)} fusion(bf16[2048,3072]{0,1:T(8,128)(2,1)} %constant_dynamic-update-slice_fusion, bf16[1024,2048]{1,0:T(8,128)(2,1)S(1)} %copy-done.1, f32[1024]{0:T(1024)S(1)} %add_rsqrt_fusion), kind=kOutput, calls=%fused_computation.5 | convolution fusion | flops 12891193344 | bytes 29364224 | tf_op jit(solution)/shard_map/dot_general | solution.py:55
  272.5 4.5 fusion.5
  277.0 4.5 fusion.6
  281.7 2.0 copy.22
  285.0 2.7 dynamic-slice_bitcast_fusion
  287.7 23.1 %all-gather.5.cloned.1.call-done = bf16[2,1024,768]{1,0,2:T(2,128)(2,1)} async-done(((bf16[2,1024,192]{1,0,2:T(2,128)(2,1)}), bf16[2,1024,768]{1,0,2:T(2,128)(2,1)}) %all-gather.5.cloned.1.call-update) | async-done | bytes 3145744 | tf_op jit(solution)/shard_map/all_gather | solution.py:63
  310.8 7.8 %fusion.7 = (bf16[1,1024,768]{1,0,2:T(2,128)(2,1)S(1)}, bf16[1,1024,768]{1,0,2:T(2,128)(2,1)S(1)}) fusion(bf16[2,1024,768]{1,0,2:T(2,128)(2,1)} %all-gather.5.cloned.1.call-done), kind=kLoop, calls=%fused_computation.55 | loop fusion | bytes 6291456 | tf_op jit(solution)/shard_map/slice | solution.py:73
  319.8 92.5 %all-gather.3.cloned.1.call-done = bf16[6144,512]{1,0:T(8,128)(2,1)} async-done(((bf16[768,512]{1,0:T(8,128)(2,1)}), bf16[6144,512]{1,0:T(8,128)(2,1)}) %all-gather.3.cloned.1.call-update) | async-done | bytes 6291472 | tf_op jit(solution)/shard_map/all_gather | solution.py:38
  413.5 2.4 copy.30
  416.4 7.3 %reduce.32 = bf16[768,512]{1,0:T(8,128)(2,1)} reduce(bf16[768,1,512]{2,1,0:T(2,128)(2,1)} %bitcast.36, bf16[]{:T(256)} %broadcast.133), dimensions={1}, to_apply=%bitcast.32.reduce_sub_computation | reduce | bytes 1572866
  423.7 2.4 reshape.117
  426.0 4.4 all-to-all-start
  430.5 1.9 select_select_fusion
  432.3 9.9 %convolution_convert_fusion = bf16[1024,512]{1,0:T(8,128)(2,1)} fusion(bf16[1024,6144]{0,1:T(8,128)(2,1)S(1)} %bitcast.33, bf16[6144,512]{1,0:T(8,128)(2,1)} %all-gather.3.cloned.1.call-done), kind=kOutput, calls=%fused_computation.10 | convolution fusion | flops 6442975232 | bytes 19922944 | tf_op jit(solution)/shard_map/dot_general | solution.py:75
  442.2 2.4 reshape.118
  (43 shorter events, 12.2 us)
Async XLA Ops:
  7.2 145.6 %copy-start.6 = (f32[1024,2]{0,1:T(2,128)S(1)}, f32[1024,2]{0,1:T(2,128)}, u32[]{:S(2)}) copy-start(f32[1024,2]{0,1:T(2,128)} %param.13) | copy-start | bytes 24580
  7.2 145.6 %copy-start.5 = (s32[1024,2]{0,1:T(2,128)S(1)}, s32[1024,2]{0,1:T(2,128)}, u32[]{:S(2)}) copy-start(s32[1024,2]{0,1:T(2,128)} %param.12) | copy-start | bytes 24580
  7.2 303.6 %all-gather.5.cloned.1.call-start = ((), (), s32[]{:S(2)}) async-start(), calls=%async_computation.2 | async-start | bytes 3932160 | tf_op jit(solution)/shard_map/all_gather | solution.py:63
  7.2 144.5 %copy-start = (bf16[1024,2048]{1,0:T(8,128)(2,1)S(1)}, bf16[1024,2048]{1,0:T(8,128)(2,1)}, u32[]{:S(2)}) copy-start(bf16[1024,2048]{1,0:T(8,128)(2,1)} %param.7) | copy-start | bytes 12582916
  9.8 70.4 %collective-permute-start = (bf16[256,3072]{0,1:T(8,128)(2,1)S(1)}, bf16[256,3072]{0,1:T(8,128)(2,1)S(1)}, u32[]{:S(2)}, u32[]{:S(2)}) collective-permute-start(bf16[256,3072]{0,1:T(8,128)(2,1)S(1)} %bitcast.38), channel_id=1, source_target_pairs={{0,4},{4,8},{8,12},{12,16},{16,20},{20,24},{24,28},{28,0},{1,5},{5... | collective-permute-start | bytes 4718600 | tf_op jit(solution)/shard_map/ppermute | solution.py:29
  12.8 69.8 %collective-permute-start.1 = (bf16[256,3072]{0,1:T(8,128)(2,1)S(1)}, bf16[256,3072]{0,1:T(8,128)(2,1)S(1)}, u32[]{:S(2)}, u32[]{:S(2)}) collective-permute-start(bf16[256,3072]{0,1:T(8,128)(2,1)S(1)} %bitcast.39), channel_id=1, source_target_pairs={{0,28},{4,0},{8,4},{12,8},{16,12},{20,16},{24,20},{28,24},{1,29},{... | collective-permute-start | bytes 4718600 | tf_op jit(solution)/shard_map/ppermute | solution.py:34
  80.2 2.5 copy-start.3
  80.2 69.0 %collective-permute-start.2 = (bf16[256,3072]{0,1:T(8,128)(2,1)S(1)}, bf16[256,3072]{0,1:T(8,128)(2,1)}, u32[]{:S(2)}, u32[]{:S(2)}) collective-permute-start(bf16[256,3072]{0,1:T(8,128)(2,1)S(1)} %collective-permute-done), channel_id=1, source_target_pairs={{0,4},{4,8},{8,12},{12,16},{16,20},{20,24},{24,28},{28,0},{1,5},{5... | collective-permute-start | bytes 4718600 | tf_op jit(solution)/shard_map/ppermute | solution.py:29
  82.6 77.9 %collective-permute-start.3 = (bf16[256,3072]{0,1:T(8,128)(2,1)S(1)}, bf16[256,3072]{0,1:T(8,128)(2,1)}, u32[]{:S(2)}, u32[]{:S(2)}) collective-permute-start(bf16[256,3072]{0,1:T(8,128)(2,1)S(1)} %collective-permute-done.1), channel_id=1, source_target_pairs={{0,28},{4,0},{8,4},{12,8},{16,12},{20,16},{24,20},{28,24},{1,29},{... | collective-permute-start | bytes 4718600 | tf_op jit(solution)/shard_map/ppermute | solution.py:34
  149.1 68.6 %collective-permute-start.4 = (bf16[256,3072]{0,1:T(8,128)(2,1)}, bf16[256,3072]{0,1:T(8,128)(2,1)}, u32[]{:S(2)}, u32[]{:S(2)}) collective-permute-start(bf16[256,3072]{0,1:T(8,128)(2,1)} %collective-permute-done.2), channel_id=1, source_target_pairs={{0,4},{4,8},{8,12},{12,16},{16,20},{20,24},{24,28},{28,0},{1,5},{5... | collective-permute-start | bytes 4718600 | tf_op jit(solution)/shard_map/ppermute | solution.py:29
  153.0 10.6 %copy-start.4 = (bf16[256,3072]{0,1:T(8,128)(2,1)S(1)}, bf16[256,3072]{0,1:T(8,128)(2,1)}, u32[]{:S(2)}) copy-start(bf16[256,3072]{0,1:T(8,128)(2,1)} %copy-done.3) | copy-start | bytes 4718596
  160.6 69.4 %collective-permute-start.5 = (bf16[256,3072]{0,1:T(8,128)(2,1)}, bf16[256,3072]{0,1:T(8,128)(2,1)S(1)}, u32[]{:S(2)}, u32[]{:S(2)}) collective-permute-start(bf16[256,3072]{0,1:T(8,128)(2,1)} %collective-permute-done.3), channel_id=1, source_target_pairs={{0,28},{4,0},{8,4},{12,8},{16,12},{20,16},{24,20},{28,24},{1,29},{... | collective-permute-start | bytes 4718600 | tf_op jit(solution)/shard_map/ppermute | solution.py:34
  217.7 37.6 %collective-permute-start.6 = (bf16[256,3072]{0,1:T(8,128)(2,1)}, bf16[256,3072]{0,1:T(8,128)(2,1)S(1)}, u32[]{:S(2)}, u32[]{:S(2)}) collective-permute-start(bf16[256,3072]{0,1:T(8,128)(2,1)} %collective-permute-done.4), channel_id=1, source_target_pairs={{0,4},{4,8},{8,12},{12,16},{16,20},{20,24},{24,28},{28,0},{1,5},{5... | collective-permute-start | bytes 4718600 | tf_op jit(solution)/shard_map/ppermute | solution.py:29
  224.3 32.3 %copy-start.1 = (bf16[1024,2048]{1,0:T(8,128)(2,1)S(1)}, bf16[1024,2048]{1,0:T(8,128)(2,1)}, u32[]{:S(2)}) copy-start(bf16[1024,2048]{1,0:T(8,128)(2,1)} %param.7) | copy-start | bytes 12582916
  277.0 7.0 %copy-start.2 = (f32[8,96,512]{2,1,0:T(8,128)S(1)}, f32[8,96,512]{2,1,0:T(8,128)}, u32[]{:S(2)}) copy-start(f32[8,96,512]{2,1,0:T(8,128)} %param.11) | copy-start | bytes 4718596
  283.8 128.5 %all-gather.3.cloned.1.call-start = ((), (), s32[]{:S(2)}) async-start(), calls=%async_computation.1 | async-start | bytes 7077888 | tf_op jit(solution)/shard_map/all_gather | solution.py:38
  426.0 16.2 %all-to-all-start = ((bf16[4,2,49152]{2,1,0:T(2,128)(2,1)}), bf16[4,2,49152]{2,1,0:T(2,128)(2,1)}, u32[]{:S(2)}, u32[]{:S(2)}) async-start(bf16[4,2,49152]{2,1,0:T(2,128)(2,1)} %reshape.117), calls=%async_computation | async-start | bytes 1572864 | tf_op jit(solution)/shard_map/all_to_all | solution.py:85
Sparse Core Ops, SparseCore 0:
  283.9 26.8 all-gather.4
  313.6 98.6 all-gather.2
